TPU v7x, 32 devices: a whole 2x2x4 slice. The times are simulated.
32 devices in a mesh: ep: 32 (over z, y, x, core).
Axes of the slice: x: 2, y: 2, z: 4, core: 2. Of those that a mesh axis runs over, the one named last changes fastest.
Arguments:
- tokens: bfloat16 [512, 2048], P('ep'), may hold values from -6 to 6
- cache_keys: bfloat16 [512, 1024, 128], P('ep'), may hold values from -6 to 6
- cache_values: bfloat16 [512, 1024, 128], P('ep'), may hold values from -6 to 6
- cache_len: int32 [512], P('ep'), may hold values from 1 to 1024
- norm_gain_first: float32 [2048], replicated, may hold values from 0.1 to 1.9
- w_query: bfloat16 [2048, 2048], P(None, 'ep'), may hold values from -0.125 to 0.125
- w_key: bfloat16 [2048, 128], replicated, may hold values from -0.125 to 0.125
- w_value: bfloat16 [2048, 128], replicated, may hold values from -0.125 to 0.125
- head_bias: float32 [32], replicated, may hold values from -8.5 to -3
- w_output: bfloat16 [2048, 2048], P(None, 'ep'), may hold values from -0.125 to 0.125
- norm_gain_second: float32 [2048], replicated, may hold values from 0.1 to 1.9
- group_id: int32 [512], P('ep'), may hold values from 0 to 1, as said below
- member: int32 [512, 6], P('ep'), may hold values from 0 to 15, as said below
- group_gate: float32 [512], P('ep'), may hold values from 0.3 to 1
- member_weight: float32 [512, 6], P('ep'), may hold values from 0.05 to 0.5
- expert_gate_w: bfloat16 [32, 2048, 512], P('ep'), may hold values from -0.125 to 0.125
- expert_up_w: bfloat16 [32, 2048, 512], P('ep'), may hold values from -0.125 to 0.125
- expert_down_w: bfloat16 [32, 512, 2048], P('ep'), may hold values from -0.25 to 0.25
- dense_gate_w: bfloat16 [2048, 2048], P(None, 'ep'), may hold values from -0.125 to 0.125
- dense_up_w: bfloat16 [2048, 2048], P(None, 'ep'), may hold values from -1 to 1
- hidden_gain: float32 [2048], replicated, may hold values from 0.1 to 1.9
- dense_down_w: bfloat16 [2048, 2048], P(None, 'ep'), may hold values from -0.125 to 0.125
- branch_logit: float32 [2048], replicated, may hold values from -8 to 8
Outputs:
- mixed_out: bfloat16 [512, 2048], P('ep')
- new_keys: bfloat16 [512, 128], P('ep')
- new_values: bfloat16 [512, 128], P('ep')
Inputs may be any that keep to these rules, and one draw needn't show every extreme that they name: `group_id`: each group number is named by exactly 8 of the tokens of one device. `member`: each row names 6 different members; with group_id, no expert is named by more than 8 tokens of one device, and some expert is named by 8 tokens of every device.
All inputs are finite; a program needn't handle non-finite values.
Results may differ from a plain program's by a relative error of at most 0.0085.
Values may be sent and summed in bfloat16 or wider, within the bound.
A program may use at most 128 MiB of HBM per device.

v0:
```python
import jax
import jax.numpy as jnp
from jax import lax
from jax.sharding import PartitionSpec as P

D = 2048
HEADS = 32
HEAD_DIM = 64
KV_HEADS = 2
PER_GROUP = 16
TOP_K = 6


epsilon = 1e-06


def rms_scale(values):
    return lax.rsqrt(jnp.mean(values * values, axis=-1, keepdims=True) + epsilon)


def later_sum(log_remain):
    span_len = log_remain.shape[-1]
    block_len = min(128, span_len)
    block_count = span_len // block_len
    lead = log_remain.shape[:-1]
    blocked = log_remain.reshape(lead + (block_count, block_len))
    inner = jnp.arange(block_len, dtype=jnp.int32)
    inner_after = (inner[:, None] > inner[None, :]).astype(jnp.float32)
    within = jnp.einsum("abcnj,js->abcns", blocked, inner_after, precision=lax.Precision.HIGHEST)
    totals = jnp.sum(blocked, axis=-1)
    outer = jnp.arange(block_count, dtype=jnp.int32)
    outer_after = (outer[:, None] > outer[None, :]).astype(jnp.float32)
    carried = jnp.einsum("abcj,jn->abcn", totals, outer_after, precision=lax.Precision.HIGHEST)
    return (within + carried[..., None]).reshape(lead + (span_len,))


def stick_read(queries, key_cache, value_cache, lengths, head_bias):
    batch_size = queries.shape[0]
    span_len = key_cache.shape[1]
    group_size = HEADS // KV_HEADS
    query_heads = queries.reshape(batch_size, KV_HEADS, group_size, HEAD_DIM)
    key_heads = key_cache.reshape(batch_size, span_len, KV_HEADS, HEAD_DIM)
    value_heads = value_cache.reshape(batch_size, span_len, KV_HEADS, HEAD_DIM)
    scores = jnp.einsum(
        "bkgd,bskd->bkgs", query_heads, key_heads, preferred_element_type=jnp.float32
    ) * HEAD_DIM ** (-0.5)
    scores = scores + head_bias.reshape(KV_HEADS, group_size)[None, :, :, None]
    live_mask = (jnp.arange(span_len, dtype=jnp.int32)[None, :] < lengths[:, None])[
        :, None, None, :
    ]
    log_remain = jnp.where(live_mask, jax.nn.log_sigmoid(-scores), 0.0)
    remain_after = later_sum(log_remain)
    weights = jnp.where(live_mask, jnp.exp(jax.nn.log_sigmoid(scores) + remain_after), 0.0).astype(
        jnp.bfloat16
    )
    mixed_heads = jnp.einsum(
        "bkgs,bskd->bkgd", weights, value_heads, preferred_element_type=jnp.float32
    )
    return mixed_heads.reshape(batch_size, HEADS * HEAD_DIM).astype(jnp.bfloat16)


def expert_apply(flat_rows, gate_w, up_w, down_w):
    gate_pre = jnp.dot(flat_rows, gate_w, preferred_element_type=jnp.float32)
    upper_pre = jnp.dot(flat_rows, up_w, preferred_element_type=jnp.float32)
    hidden = (jax.nn.silu(gate_pre) * upper_pre).astype(jnp.bfloat16)
    return jnp.dot(hidden, down_w, preferred_element_type=jnp.float32).astype(jnp.bfloat16)


def shards(
    tokens,
    cache_keys,
    cache_values,
    cache_len,
    norm_gain_first,
    w_query,
    w_key,
    w_value,
    head_bias,
    w_output,
    norm_gain_second,
    group_id,
    member,
    group_gate,
    member_weight,
    expert_gate_w,
    expert_up_w,
    expert_down_w,
    dense_gate_w,
    dense_up_w,
    hidden_gain,
    dense_down_w,
    branch_logit,
):
    devices = lax.axis_size("ep")
    seq_dev = tokens.shape[0]
    stream = tokens.astype(jnp.float32)
    normed_first = (stream * rms_scale(stream) * norm_gain_first).astype(jnp.bfloat16)
    new_keys = jnp.dot(normed_first, w_key, preferred_element_type=jnp.float32).astype(jnp.bfloat16)
    new_values = jnp.dot(normed_first, w_value, preferred_element_type=jnp.float32).astype(
        jnp.bfloat16
    )
    query_cols = jnp.dot(
        lax.all_gather(normed_first, "ep", axis=0, tiled=True),
        w_query,
        preferred_element_type=jnp.float32,
    ).astype(jnp.bfloat16)
    queries = lax.all_to_all(query_cols, "ep", split_axis=0, concat_axis=1, tiled=True)
    attended = stick_read(queries, cache_keys, cache_values, cache_len, head_bias)
    output_cols = jnp.dot(
        lax.all_gather(attended, "ep", axis=0, tiled=True),
        w_output,
        preferred_element_type=jnp.float32,
    ).astype(jnp.bfloat16)
    projected = lax.all_to_all(output_cols, "ep", split_axis=0, concat_axis=1, tiled=True)
    second_stream = stream + projected.astype(jnp.float32)
    normed_second = (second_stream * rms_scale(second_stream) * norm_gain_second).astype(
        jnp.bfloat16
    )
    experts = devices * expert_gate_w.shape[0]
    capacity = seq_dev // (experts // PER_GROUP)
    pair_expert = (group_id[:, None] * PER_GROUP + member).reshape(-1)
    pair_count = pair_expert.shape[0]
    expert_hits = (pair_expert[:, None] == jnp.arange(experts, dtype=jnp.int32)[None, :]).astype(
        jnp.float32
    )
    earlier = (jnp.arange(pair_count)[:, None] > jnp.arange(pair_count)[None, :]).astype(
        jnp.float32
    )
    before = jnp.dot(earlier, expert_hits, preferred_element_type=jnp.float32)
    slot_index = jnp.sum(before * expert_hits, axis=1).astype(jnp.int32)
    target = pair_expert * capacity + slot_index
    select = (jnp.arange(experts * capacity, dtype=jnp.int32)[:, None] == target[None, :]).astype(
        jnp.bfloat16
    )
    pair_rows = jnp.repeat(normed_second, TOP_K, axis=0)
    packed = jnp.dot(select, pair_rows, preferred_element_type=jnp.float32).astype(jnp.bfloat16)
    packed = packed.reshape(experts, capacity, D)
    received = lax.all_to_all(packed, "ep", split_axis=0, concat_axis=0, tiled=True)
    flat_rows = received.reshape(-1, received.shape[-1])
    result_rows = expert_apply(flat_rows, expert_gate_w[0], expert_up_w[0], expert_down_w[0])
    served = result_rows.reshape(received.shape)
    returned = lax.all_to_all(served, "ep", split_axis=0, concat_axis=0, tiled=True).reshape(
        experts * capacity, D
    )
    pair_out = lax.dot_general(
        select, returned, (((0,), (0,)), ((), ())), preferred_element_type=jnp.float32
    )
    combine = (group_gate[:, None] * member_weight).reshape(-1, 1)
    routed = jnp.sum((pair_out * combine).reshape(seq_dev, TOP_K, D), axis=1)
    gathered = lax.all_gather(normed_second, "ep", axis=0, tiled=True)
    dense_gate = jnp.dot(gathered, dense_gate_w, preferred_element_type=jnp.float32)
    dense_upper = jnp.dot(gathered, dense_up_w, preferred_element_type=jnp.float32)
    dense_hidden = jax.nn.silu(dense_gate) * dense_upper
    own_hidden = lax.all_to_all(
        dense_hidden.astype(jnp.bfloat16), "ep", split_axis=0, concat_axis=1, tiled=True
    ).astype(dense_hidden.dtype)
    dense_normed = (own_hidden * rms_scale(own_hidden) * hidden_gain).astype(jnp.bfloat16)
    dense_out = jnp.dot(
        dense_normed,
        lax.all_gather(dense_down_w, "ep", axis=1, tiled=True),
        preferred_element_type=jnp.float32,
    ).astype(jnp.bfloat16)
    mixed_out = (
        second_stream + routed + jax.nn.sigmoid(branch_logit) * dense_out.astype(jnp.float32)
    )
    return (mixed_out.astype(jnp.bfloat16), new_keys, new_values)


def solution(mesh):
    in_specs = (
        P("ep", None),
        P("ep", None, None),
        P("ep", None, None),
        P("ep"),
        P(),
        P(None, "ep"),
        P(),
        P(),
        P(),
        P(None, "ep"),
        P(),
        P("ep"),
        P("ep", None),
        P("ep"),
        P("ep", None),
        P("ep", None, None),
        P("ep", None, None),
        P("ep", None, None),
        P(None, "ep"),
        P(None, "ep"),
        P(),
        P(None, "ep"),
        P(),
    )
    out_specs = (P("ep", None), P("ep", None), P("ep", None))
    return jax.shard_map(shards, mesh=mesh, in_specs=in_specs, out_specs=out_specs, check_vma=False)
```

profile of v0, /device:TPU:0, one launch (start us, length us, event | category | flops | bytes accessed | tf_op | source)
XLA Modules:
  0.0 332.1 jit_solution(780051894646307510)
XLA Ops:
  10.7 6.4 %copy.46 = bf16[16,1024,128]{1,2,0:T(8,128)(2,1)} copy(bf16[16,1024,128]{2,1,0:T(8,128)(2,1)} %param.24) | data formatting | bytes 8388608 | tf_op args[1]
  17.1 6.5 %copy.49 = bf16[16,1024,128]{1,2,0:T(8,128)(2,1)} copy(bf16[16,1024,128]{2,1,0:T(8,128)(2,1)} %param.25) | data formatting | bytes 8388608 | tf_op args[2]
  23.6 46.8 %all-gather.5.cloned.1.call-done = bf16[512,2048]{1,0:T(8,128)(2,1)} async-done(((bf16[16,2048]{1,0:T(8,128)(2,1)}), bf16[512,2048]{1,0:T(8,128)(2,1)}) %all-gather.5.cloned.1.call-update) | async-done | bytes 2097168 | tf_op jit(solution)/shard_map/all_gather | solution.py:103
  70.4 2.3 convolution_convert_fusion.5
  73.6 3.5 %all-to-all-start = ((bf16[32,2,512]{2,1,0:T(2,128)(2,1)}), bf16[32,2,512]{2,1,0:T(2,128)(2,1)S(1)}, u32[]{:S(2)}, u32[]{:S(2)}) async-start(bf16[32,2,512]{2,1,0:T(2,128)(2,1)} %reshape.136), calls=%async_computation | async-start | bytes 131072 | tf_op jit(solution)/shard_map/all_to_all | solution.py:107
  77.2 7.3 %all-to-all-done = bf16[32,2,512]{2,1,0:T(2,128)(2,1)S(1)} async-done(((bf16[32,2,512]{2,1,0:T(2,128)(2,1)}), bf16[32,2,512]{2,1,0:T(2,128)(2,1)S(1)}, u32[]{:S(2)}, u32[]{:S(2)}) %all-to-all-start) | async-done | bytes 65568 | tf_op jit(solution)/shard_map/all_to_all | solution.py:107
  84.7 5.1 %fusion.12 = (f32[16,2,16,1024]{3,2,1,0:T(8,128)S(1)}, f32[16,2,16,1024]{3,2,1,0:T(8,128)}) fusion(f32[2,16]{1,0:T(2,128)S(1)} %add.89, pred[16,1024]{1,0:T(8,128)(4,1)S(1)} %iota_compare_fusion.4, bf16[16,2,16,64]{3,2,1,0:T(8,128)(2,1)S(1)} %bitcast.87, bf16[16,1024,2,64]{1,3,2,0:T(8,128)(2,1)} %bitcast.81), kind=kOutput, calls=%fused_computation.18 | convolution fusion | flops 72351744 | bytes 8470656 | tf_op jit(solution)/shard_map/bkgd,bskd->bkgs/dot_general | solution.py:44
  91.6 2.2 reduce_sum.55
  94.1 4.1 %convolution_add_fusion = f32[16,2,16,8,128]{4,3,2,1,0:T(8,128)} fusion(f32[16,2,16,8,128]{4,3,2,1,0:T(8,128)} %bitcast.79, f32[16,2,16,8]{3,2,1,0:T(8,128)S(1)} %fusion.55), kind=kOutput, calls=%fused_computation.25 | convolution fusion | flops 805847040 | bytes 4210688 | tf_op jit(solution)/shard_map/abcnj,js->abcns/dot_general | solution.py:29
  98.2 2.7 reshape.123
  100.9 5.5 %convolution_convert_fusion.3 = bf16[16,2,16,64]{3,2,1,0:T(8,128)(2,1)S(1)} fusion(bf16[16,1024,2,64]{1,3,2,0:T(8,128)(2,1)} %bitcast.80, f32[16,2,16,1024]{3,2,1,0:T(8,128)} %reshape.123, f32[16,2,16,1024]{3,2,1,0:T(8,128)} %get-tuple-element.4, f32[2,16]{1,0:T(2,128)S(1)} %add.89, pred[16,1024]{1,0:T(8,128)(4,1)S(1)} %iota_compare_fusion.4), kind=kOutput, calls=%fused_computation.28 | convolution fusion | flops 73957376 | bytes 8470656 | tf_op jit(solution)/shard_map/bkgs,bskd->bkgd/dot_general | solution.py:56
  107.3 53.0 %all-gather.7.cloned.1.call-done = bf16[512,2048]{1,0:T(8,128)(2,1)} async-done(((bf16[16,2048]{1,0:T(8,128)(2,1)}), bf16[512,2048]{1,0:T(8,128)(2,1)}) %all-gather.7.cloned.1.call-update) | async-done | bytes 2097168 | tf_op jit(solution)/shard_map/all_gather | solution.py:110
  160.3 2.3 convolution_convert_fusion.4
  162.9 10.7 %all_to_all.52 = bf16[32,2,512]{2,1,0:T(2,128)(2,1)S(1)} all-to-all(bf16[32,2,512]{2,1,0:T(2,128)(2,1)S(1)} %reshape.138), channel_id=1, replica_groups=mesh['ep'=32] {'ep'}, dimensions={0} | all-to-all | bytes 131072 | tf_op jit(solution)/shard_map/all_to_all | solution.py:114
  177.4 30.7 %all_to_all.53 = bf16[32,8,2048]{2,1,0:T(8,128)(2,1)S(1)} all-to-all(bf16[32,8,2048]{2,1,0:T(8,128)(2,1)S(1)} %fusion), channel_id=1, replica_groups=mesh['ep'=32] {'ep'}, dimensions={0} | all-to-all | bytes 2097152 | tf_op jit(solution)/shard_map/all_to_all | solution.py:138
  209.6 4.0 %fusion.1 = bf16[32,8,2048]{2,1,0:T(8,128)(2,1)} fusion(bf16[1,512,2048]{2,1,0:T(8,128)(2,1)S(1)} %copy-done, bf16[1,2048,512]{2,1,0:T(8,128)(2,1)} %param.39, bf16[32,8,2048]{2,1,0:T(8,128)(2,1)S(1)} %all_to_all.53, f32[256,512]{1,0:T(8,128)} %fusion.16), kind=kOutput, calls=%fused_computation.5 | convolution fusion | flops 1075052544 | bytes 6815744 | tf_op jit(solution)/shard_map/dot_general | solution.py:66
  213.6 3.7 %all-to-all-start.3 = ((bf16[32,8,2048]{2,1,0:T(8,128)(2,1)}), bf16[32,8,2048]{2,1,0:T(8,128)(2,1)S(1)}, u32[]{:S(2)}, u32[]{:S(2)}) async-start(bf16[32,8,2048]{2,1,0:T(8,128)(2,1)} %fusion.1), calls=%async_computation.3 | async-start | bytes 2097152 | tf_op jit(solution)/shard_map/all_to_all | solution.py:142
  221.2 18.6 %all-gather.9.cloned.1.call-done = bf16[512,2048]{1,0:T(8,128)(2,1)} async-done(((bf16[16,2048]{1,0:T(8,128)(2,1)}), bf16[512,2048]{1,0:T(8,128)(2,1)}) %all-gather.9.cloned.1.call-update) | async-done | bytes 2097168 | tf_op jit(solution)/shard_map/all_gather | solution.py:150
  239.9 2.5 fusion.60
  244.0 5.0 %all-to-all-done.3 = bf16[32,8,2048]{2,1,0:T(8,128)(2,1)S(1)} async-done(((bf16[32,8,2048]{2,1,0:T(8,128)(2,1)}), bf16[32,8,2048]{2,1,0:T(8,128)(2,1)S(1)}, u32[]{:S(2)}, u32[]{:S(2)}) %all-to-all-start.3) | async-done | bytes 1048608 | tf_op jit(solution)/shard_map/all_to_all | solution.py:142
  249.0 3.6 %all-to-all-start.4 = ((bf16[32,2,512]{2,1,0:T(2,128)(2,1)}), bf16[32,2,512]{2,1,0:T(2,128)(2,1)S(1)}, u32[]{:S(2)}, u32[]{:S(2)}) async-start(bf16[32,2,512]{2,1,0:T(2,128)(2,1)} %reshape.140), calls=%async_computation.4 | async-start | bytes 131072 | tf_op jit(solution)/shard_map/all_to_all | solution.py:154
  255.5 5.1 %all-to-all-done.4 = bf16[32,2,512]{2,1,0:T(2,128)(2,1)S(1)} async-done(((bf16[32,2,512]{2,1,0:T(2,128)(2,1)}), bf16[32,2,512]{2,1,0:T(2,128)(2,1)S(1)}, u32[]{:S(2)}, u32[]{:S(2)}) %all-to-all-start.4) | async-done | bytes 65568 | tf_op jit(solution)/shard_map/all_to_all | solution.py:154
  261.2 58.1 %all-gather.11.cloned.1.call-done = bf16[2048,2048]{0,1:T(8,128)(2,1)} async-done(((bf16[2048,64]{0,1:T(8,128)(2,1)}), bf16[2048,2048]{0,1:T(8,128)(2,1)}) %all-gather.11.cloned.1.call-update) | async-done | bytes 8388624 | tf_op jit(solution)/shard_map/all_gather | solution.py:160
  319.3 6.3 %fusion.5 = bf16[16,2048]{1,0:T(8,128)(2,1)} fusion(bf16[2048,2048]{0,1:T(8,128)(2,1)} %all-gather.11.cloned.1.call-done, f32[16,2048]{1,0:T(8,128)S(1)} %reduce_sum.58, f32[16,2048]{1,0:T(8,128)S(1)} %reshape.133, f32[2048]{0:T(1024)S(1)} %copy-done.6, f32[16]{0:T(128)S(1)} %add_rsqrt_fusion, f32[2048]{0:T(1024)S(1)} %add_divide_fusion, ...), kind=kOutput, calls=%fused_computation.11 | convolution fusion | flops 134578176 | bytes 8929344 | tf_op jit(solution)/shard_map/dot_general | solution.py:158
  (89 shorter events, 21.9 us)
Async XLA Ops:
  7.2 202.4 %copy-start = (bf16[1,512,2048]{2,1,0:T(8,128)(2,1)S(1)}, bf16[1,512,2048]{2,1,0:T(8,128)(2,1)}, u32[]{:S(2)}) copy-start(bf16[1,512,2048]{2,1,0:T(8,128)(2,1)} %param.40) | copy-start | bytes 6291460
  7.2 63.2 %all-gather.5.cloned.1.call-start = ((), (), s32[]{:S(2)}) async-start(), calls=%async_computation.5 | async-start | bytes 2162688 | tf_op jit(solution)/shard_map/all_gather | solution.py:103
  17.1 53.3 %copy-start.4 = (bf16[2048,64]{0,1:T(8,128)(2,1)S(1)}, bf16[2048,64]{0,1:T(8,128)(2,1)}, u32[]{:S(2)}) copy-start(bf16[2048,64]{0,1:T(8,128)(2,1)} %param.28) | copy-start | bytes 786436
  23.6 53.6 %copy-start.11 = (s32[16]{0:T(128)S(1)}, s32[16]{0:T(128)}, u32[]{:S(2)}) copy-start(s32[16]{0:T(128)} %param.26) | copy-start | bytes 196
  73.6 10.9 %all-to-all-start = ((bf16[32,2,512]{2,1,0:T(2,128)(2,1)}), bf16[32,2,512]{2,1,0:T(2,128)(2,1)S(1)}, u32[]{:S(2)}, u32[]{:S(2)}) async-start(bf16[32,2,512]{2,1,0:T(2,128)(2,1)} %reshape.136), calls=%async_computation | async-start | bytes 131072 | tf_op jit(solution)/shard_map/all_to_all | solution.py:107
  77.1 83.2 %all-gather.7.cloned.1.call-start = ((), (), s32[]{:S(2)}) async-start(), calls=%async_computation.6 | async-start | bytes 2162688 | tf_op jit(solution)/shard_map/all_gather | solution.py:110
  100.9 59.4 %copy-start.5 = (bf16[2048,64]{0,1:T(8,128)(2,1)S(1)}, bf16[2048,64]{0,1:T(8,128)(2,1)}, u32[]{:S(2)}) copy-start(bf16[2048,64]{0,1:T(8,128)(2,1)} %param.32) | copy-start | bytes 786436
  107.2 66.8 %copy-start.2 = (bf16[16,2048]{1,0:T(8,128)(2,1)S(1)}, bf16[16,2048]{1,0:T(8,128)(2,1)}, u32[]{:S(2)}) copy-start(bf16[16,2048]{1,0:T(8,128)(2,1)} %param.23) | copy-start | bytes 196612
  107.2 66.9 %copy-start.7 = (f32[2048]{0:T(1024)S(1)}, f32[2048]{0:T(1024)}, u32[]{:S(2)}) copy-start(f32[2048]{0:T(1024)} %param.33) | copy-start | bytes 24580
  107.2 68.2 %copy-start.15 = (s32[16]{0:T(128)S(1)}, s32[16]{0:T(128)}, u32[]{:S(2)}) copy-start(s32[16]{0:T(128)} %param.34) | copy-start | bytes 196
  107.3 68.2 %copy-start.9 = (s32[16,6]{0,1:T(8,128)S(1)}, s32[16,6]{0,1:T(8,128)}, u32[]{:S(2)}) copy-start(s32[16,6]{0,1:T(8,128)} %param.35) | copy-start | bytes 1156
  107.3 132.6 %all-gather.9.cloned.1.call-start = ((), (), s32[]{:S(2)}) async-start(), calls=%async_computation.7 | async-start | bytes 2162688 | tf_op jit(solution)/shard_map/all_gather | solution.py:150
  174.9 144.4 %all-gather.11.cloned.1.call-start = ((), (), s32[]{:S(2)}) async-start(), calls=%async_computation.8 | async-start | bytes 8650752 | tf_op jit(solution)/shard_map/all_gather | solution.py:160
  176.9 31.2 %copy-start.13 = (bf16[1,2048,512]{2,1,0:T(8,128)(2,1)S(1)}, bf16[1,2048,512]{2,1,0:T(8,128)(2,1)}, u32[]{:S(2)}) copy-start(bf16[1,2048,512]{2,1,0:T(8,128)(2,1)} %param.38) | copy-start | bytes 6291460
  213.6 3.7 %copy-start.10 = (f32[16,6]{0,1:T(8,128)S(1)}, f32[16,6]{0,1:T(8,128)}, u32[]{:S(2)}) copy-start(f32[16,6]{0,1:T(8,128)} %param.37) | copy-start | bytes 1156
  213.6 3.7 %copy-start.12 = (f32[16]{0:T(128)S(1)}, f32[16]{0:T(128)}, u32[]{:S(2)}) copy-start(f32[16]{0:T(128)} %param.36) | copy-start | bytes 196
  213.6 3.9 %copy-start.8 = (f32[2048]{0:T(1024)S(1)}, f32[2048]{0:T(1024)}, u32[]{:S(2)}) copy-start(f32[2048]{0:T(1024)} %param.45) | copy-start | bytes 24580
  213.6 4.0 %copy-start.3 = (bf16[16,2048]{1,0:T(8,128)(2,1)S(1)}, bf16[16,2048]{1,0:T(8,128)(2,1)}, u32[]{:S(2)}) copy-start(bf16[16,2048]{1,0:T(8,128)(2,1)} %fusion.46) | copy-start | bytes 196612
  213.6 35.4 %all-to-all-start.3 = ((bf16[32,8,2048]{2,1,0:T(8,128)(2,1)}), bf16[32,8,2048]{2,1,0:T(8,128)(2,1)S(1)}, u32[]{:S(2)}, u32[]{:S(2)}) async-start(bf16[32,8,2048]{2,1,0:T(8,128)(2,1)} %fusion.1), calls=%async_computation.3 | async-start | bytes 2097152 | tf_op jit(solution)/shard_map/all_to_all | solution.py:142
  239.9 2.5 copy-start.1
  239.9 2.5 copy-start.14
  249.0 11.6 %all-to-all-start.4 = ((bf16[32,2,512]{2,1,0:T(2,128)(2,1)}), bf16[32,2,512]{2,1,0:T(2,128)(2,1)S(1)}, u32[]{:S(2)}, u32[]{:S(2)}) async-start(bf16[32,2,512]{2,1,0:T(2,128)(2,1)} %reshape.140), calls=%async_computation.4 | async-start | bytes 131072 | tf_op jit(solution)/shard_map/all_to_all | solution.py:154
  253.9 65.3 %copy-start.6 = (f32[2048]{0:T(1024)S(1)}, f32[2048]{0:T(1024)}, u32[]{:S(2)}) copy-start(f32[2048]{0:T(1024)} %param.43) | copy-start | bytes 24580
Sparse Core Ops, SparseCore 0:
  11.4 58.9 all-gather.4
  107.3 52.9 all-gather.6
  175.0 64.7 all-gather.8
  242.6 76.6 all-gather.10
where the time goes:
time: 333 us; the launch traced here: 332 us
  waiting for transfers between devices  194 us (58%)
  blocking collectives  41.4 us (12%)
  matrix products  40.2 us (12%)
  local copies, waits for them, and re-layouts  24.6 us (7%)
  between operations  14.1 us (4%)
  starting transfers between devices  10.9 us (3%)
  other arithmetic  6.37 us (2%)
    all_gather x1, waiting for transfers between devices, shards(): lax.all_gather(dense_down_w, 'ep', axis=1, tiled=True)  58.1 us
    all_gather x1, waiting for transfers between devices, shards(): lax.all_gather(attended, 'ep', axis=0, tiled=True)  53 us
    all_gather x1, waiting for transfers between devices, shards(): lax.all_gather(normed_first, 'ep', axis=0, tiled=True)  46.8 us
    all_to_all x1, blocking collectives, shards(): lax.all_to_all(packed, 'ep', split_axis=0, concat_axis=0, tiled=True)  30.7 us
    all_gather x1, waiting for transfers between devices, shards(): gathered = lax.all_gather(normed_second, 'ep', axis=0, tiled=True)  18.6 us
    unnamed x41, local copies, waits for them, and re-layouts  16.9 us
    all_to_all x1, blocking collectives, shards(): lax.all_to_all(output_cols, 'ep', split_axis=0, concat_axis=1, tiled=True)  10.7 us
    all_to_all x1, waiting for transfers between devices, shards(): lax.all_to_all(query_cols, 'ep', split_axis=0, concat_axis=1, tiled=True)  7.26 us
  transfers between devices with their start and end apart: 7, of which 7 were waited for; matrix products, arithmetic and copies ran while one was open for 10% of the time, Pallas kernels for 0%

commit v1 on v0

v1 whole, which is shorter than its diff:
```python
import functools

import jax
import jax.numpy as jnp
from jax import lax
from jax.experimental import pallas as pl
from jax.experimental.pallas import tpu as pltpu
from jax.sharding import PartitionSpec as P

HEADS = 32
HEAD_DIM = 64
KV_HEADS = 2
PER_GROUP = 16
TOP_K = 6
LANES = 128
MESH = pl.DeviceIdType.MESH

epsilon = 1e-06


def torus_of(chips):
    best = (chips, 1, 1)
    for x in range(1, chips + 1):
        for y in range(x, chips + 1):
            if chips % (x * y) == 0 and chips // (x * y) >= y:
                z = chips // (x * y)
                if z + y + x < sum(best):
                    best = (z, y, x)
    return best


def rms_scale(values):
    return lax.rsqrt(jnp.mean(values * values, axis=-1, keepdims=True) + epsilon)


class Place:
    def __init__(self, chips):
        self.chips = chips
        self.dims = torus_of(chips)
        me = lax.axis_index("ep")
        self.core = lax.rem(me, 2)
        self.chip = me // 2
        depth, height, width = self.dims
        self.x = lax.rem(self.chip, width)
        self.y = lax.rem(self.chip // width, height)
        self.z = self.chip // (width * height)

    def at(self, dz, dy, dx):
        depth, height, width = self.dims
        z = lax.rem(self.z + dz + depth, depth)
        y = lax.rem(self.y + dy + height, height)
        x = lax.rem(self.x + dx + width, width)
        return (z * height + y) * width + x

    def device(self, chip):
        return (chip * 2 + self.core,)

    def greet(self):
        barrier = pltpu.get_barrier_semaphore()
        for step in range(1, self.chips):
            other = lax.rem(self.chip + step, self.chips)
            pl.semaphore_signal(barrier, inc=1, device_id=self.device(other), device_id_type=MESH)
        pl.semaphore_wait(barrier, self.chips - 1)


def spread(place, halves):
    depth, height, width = place.dims
    sent = []
    counts = [0, 0]

    def push(half, source, origin, target):
        own, slots, send, recv = halves[half]
        copy = pltpu.make_async_remote_copy(
            src_ref=own if source is None else slots.at[source],
            dst_ref=slots.at[origin],
            send_sem=send.at[counts[half]],
            recv_sem=recv.at[origin],
            device_id=place.device(target),
            device_id_type=MESH,
        )
        counts[half] += 1
        copy.start()
        sent.append(copy)

    def arrive(half, origin):
        own, slots, send, recv = halves[half]
        pltpu.make_async_remote_copy(
            src_ref=slots.at[origin],
            dst_ref=slots.at[origin],
            send_sem=send.at[0],
            recv_sem=recv.at[origin],
            device_id=place.device(place.chip),
            device_id_type=MESH,
        ).wait_recv()

    def along(half, source, origin, axis):
        if axis == "x":
            for step in range(1, width):
                push(half, source, origin, place.at(0, 0, step))
        else:
            for step in range(1, height):
                push(half, source, origin, place.at(0, step, 0))

    orders = (("x", "y"), ("y", "x"))
    for step in range(1, depth):
        for half in range(2):
            push(half, None, place.chip, place.at(step, 0, 0))
    for half in range(2):
        for axis in orders[half]:
            along(half, None, place.chip, axis)
    for step in range(1, depth):
        for half in range(2):
            origin = place.at(-step, 0, 0)
            arrive(half, origin)
            for axis in orders[half]:
                along(half, origin, origin, axis)
    for up in range(depth):
        for half in range(2):
            reach = width if half == 0 else height
            for step in range(1, reach):
                origin = place.at(-up, 0, -step) if half == 0 else place.at(-up, -step, 0)
                arrive(half, origin)
                along(half, origin, origin, orders[half][1])
    for up in range(depth):
        for half in range(2):
            for dy in range(height):
                for dx in range(width):
                    if (dy if half == 0 else dx) != 0:
                        arrive(half, place.at(-up, -dy, -dx))
    for half in range(2):
        own, slots, _, _ = halves[half]
        slots[place.chip] = own[...]
    return sent


def deliver(place, tiles, landed, send, recv, out_ref):
    copies = []
    for step in range(1, place.chips):
        other = lax.rem(place.chip + step, place.chips)
        copy = pltpu.make_async_remote_copy(
            src_ref=tiles.at[other],
            dst_ref=landed.at[place.chip],
            send_sem=send.at[step],
            recv_sem=recv.at[place.chip],
            device_id=place.device(other),
            device_id_type=MESH,
        )
        copy.start()
        copies.append(copy)
    landed[place.chip] = tiles[place.chip]
    for step in range(1, place.chips):
        origin = lax.rem(place.chip - step + place.chips, place.chips)
        pltpu.make_async_remote_copy(
            src_ref=landed.at[origin],
            dst_ref=landed.at[origin],
            send_sem=send.at[0],
            recv_sem=recv.at[origin],
            device_id=place.device(place.chip),
            device_id_type=MESH,
        ).wait_recv()
    lanes = landed.shape[2]
    for block in range(place.chips):
        out_ref[:, block * lanes : (block + 1) * lanes] = landed[block]
    for copy in copies:
        copy.wait_send()


def flat(slots):
    count, rows, columns = slots.shape
    return slots[...].reshape(count * rows, columns)


def project_kernel(chips, a_ref, b_ref, w_ref, out_ref, slots_a, slots_b, tiles, landed,
                   send_a, recv_a, send_b, recv_b, send_t, recv_t):
    place = Place(chips)
    place.greet()
    sent = spread(place, ((a_ref, slots_a, send_a, recv_a), (b_ref, slots_b, send_b, recv_b)))
    cut = a_ref.shape[1]
    product = jnp.dot(flat(slots_a), w_ref[:cut], preferred_element_type=jnp.float32)
    product = product + jnp.dot(flat(slots_b), w_ref[cut:], preferred_element_type=jnp.float32)
    tiles[...] = product.astype(jnp.bfloat16).reshape(tiles.shape)
    deliver(place, tiles, landed, send_t, recv_t, out_ref)
    for copy in sent:
        copy.wait_send()


def gather_kernel(chips, a_ref, b_ref, gate_ref, up_ref, rows_ref, notes_ref, hidden_ref, slots_a, slots_b,
                  send_a, recv_a, send_b, recv_b):
    place = Place(chips)
    place.greet()
    sent = spread(place, ((a_ref, slots_a, send_a, recv_a), (b_ref, slots_b, send_b, recv_b)))
    cut = b_ref.shape[1]
    rows_a = slots_a[:, :, :cut].reshape(chips * a_ref.shape[0], cut)
    rows_b = flat(slots_b)
    rows_ref[:, :cut] = rows_a
    rows_ref[:, cut:] = rows_b
    notes_ref[...] = slots_a[:, :, cut:].reshape(notes_ref.shape)
    gate = jnp.dot(rows_a, gate_ref[:cut], preferred_element_type=jnp.float32)
    gate = gate + jnp.dot(rows_b, gate_ref[cut:], preferred_element_type=jnp.float32)
    upper = jnp.dot(rows_a, up_ref[:cut], preferred_element_type=jnp.float32)
    upper = upper + jnp.dot(rows_b, up_ref[cut:], preferred_element_type=jnp.float32)
    hidden_ref[...] = (jax.nn.silu(gate) * upper).astype(jnp.bfloat16)
    for copy in sent:
        copy.wait_send()


def down_kernel(chips, a_ref, b_ref, gain_ref, w_ref, out_ref, slots_a, slots_b, tiles, landed,
                send_a, recv_a, send_b, recv_b, send_t, recv_t):
    place = Place(chips)
    place.greet()
    sent = spread(place, ((a_ref, slots_a, send_a, recv_a), (b_ref, slots_b, send_b, recv_b)))
    rows, lanes = a_ref.shape
    part = chips // 2
    for half, slots in enumerate((slots_a, slots_b)):
        square = jnp.zeros((rows, lanes), jnp.float32)
        for block in range(chips):
            value = slots[block].astype(jnp.float32)
            square = square + value * value
        mean = jnp.sum(square, axis=1, keepdims=True) / (chips * lanes)
        scale = lax.rsqrt(mean + epsilon)
        total = jnp.zeros((rows, lanes), jnp.float32)
        for block in range(chips):
            gain = gain_ref[:, block * lanes : (block + 1) * lanes]
            normed = (slots[block].astype(jnp.float32) * scale * gain).astype(jnp.bfloat16)
            total = total + jnp.dot(
                normed,
                w_ref[block * lanes : (block + 1) * lanes],
                preferred_element_type=jnp.float32,
            )
        tiles[half * part : (half + 1) * part] = total.astype(jnp.bfloat16).reshape(
            part, rows // part, lanes
        )
    deliver(place, tiles, landed, send_t, recv_t, out_ref)
    for copy in sent:
        copy.wait_send()


def whole():
    return pl.BlockSpec(memory_space=pltpu.VMEM)


def spread_scratch(chips, a, b):
    slots = [pltpu.VMEM((chips,) + a.shape, a.dtype), pltpu.VMEM((chips,) + b.shape, b.dtype)]
    return slots, [pltpu.SemaphoreType.DMA((chips,))] * 4


def remote_params(number):
    return pltpu.CompilerParams(collective_id=number, has_side_effects=True)


def project(chips, number, rows, weight):
    count, width = rows.shape
    lanes = weight.shape[1]
    a, b = rows[:, : width // 2], rows[:, width // 2 :]
    slots, sems = spread_scratch(chips, a, b)
    tile = pltpu.VMEM((chips, count, lanes), jnp.bfloat16)
    return pl.pallas_call(
        functools.partial(project_kernel, chips),
        out_shape=jax.ShapeDtypeStruct((count, chips * lanes), jnp.bfloat16),
        in_specs=[whole()] * 3,
        out_specs=whole(),
        scratch_shapes=slots + [tile, tile] + sems + [pltpu.SemaphoreType.DMA((chips,))] * 2,
        compiler_params=remote_params(number),
        name="project",
    )(a, b, weight)


def gather_rows(chips, number, rows, notes, gate_w, up_w):
    count, width = rows.shape
    a = jnp.concatenate([rows[:, : width // 2], notes], axis=1)
    b = rows[:, width // 2 :]
    slots, sems = spread_scratch(chips, a, b)
    return pl.pallas_call(
        functools.partial(gather_kernel, chips),
        out_shape=(
            jax.ShapeDtypeStruct((chips * count, width), jnp.bfloat16),
            jax.ShapeDtypeStruct((chips * count, LANES), jnp.bfloat16),
            jax.ShapeDtypeStruct((chips * count, gate_w.shape[1]), jnp.bfloat16),
        ),
        in_specs=[whole()] * 4,
        out_specs=(whole(),) * 3,
        scratch_shapes=slots + sems,
        compiler_params=remote_params(number),
        name="gather_rows",
    )(a, b, gate_w, up_w)


def down_project(chips, number, hidden, gain, weight):
    count, lanes = hidden.shape
    a, b = hidden[: count // 2], hidden[count // 2 :]
    slots, sems = spread_scratch(chips, a, b)
    tile = pltpu.VMEM((chips, count // chips, lanes), jnp.bfloat16)
    return pl.pallas_call(
        functools.partial(down_kernel, chips),
        out_shape=jax.ShapeDtypeStruct((count // chips, chips * lanes), jnp.bfloat16),
        in_specs=[whole()] * 4,
        out_specs=whole(),
        scratch_shapes=slots + [tile, tile] + sems + [pltpu.SemaphoreType.DMA((chips,))] * 2,
        compiler_params=remote_params(number),
        name="down_project",
    )(a, b, gain[None, :], weight)


def stick_kernel(lens_ref, q_ref, k_ref, v_ref, bias_ref, out_ref):
    step = pl.program_id(0)
    batch, span, _ = k_ref.shape
    blocks = span // LANES
    row = lax.broadcasted_iota(jnp.int32, (3 * LANES, LANES), 0)
    column = lax.broadcasted_iota(jnp.int32, (3 * LANES, LANES), 1)
    after = (lax.rem(row, LANES) > column).astype(jnp.bfloat16)
    place = lax.broadcasted_iota(jnp.int32, (HEADS, span), 1)
    bias = bias_ref[:, :1]
    group = HEADS // KV_HEADS
    head = lax.broadcasted_iota(jnp.int32, (HEADS, LANES), 0)
    lane = lax.broadcasted_iota(jnp.int32, (HEADS, LANES), 1)
    own_lanes = (head // group) == (lane // HEAD_DIM)
    late = lax.broadcasted_iota(jnp.int32, (HEADS, HEAD_DIM), 0) >= group
    for item in range(batch):
        heads = q_ref[item].astype(jnp.float32)
        heads = jnp.where(own_lanes, jnp.concatenate([heads] * KV_HEADS, axis=1), 0.0)
        scores = lax.dot_general(
            heads.astype(jnp.bfloat16), k_ref[item], (((1,), (1,)), ((), ())), preferred_element_type=jnp.float32
        )
        scores = scores * HEAD_DIM ** (-0.5) + bias
        live = place < lens_ref[step * batch + item]
        remain = -(jnp.maximum(scores, 0.0) + jnp.log1p(jnp.exp(-jnp.abs(scores))))
        log_remain = jnp.where(live, remain, 0.0)
        stacked = jnp.concatenate(
            [log_remain[:, n * LANES : (n + 1) * LANES] for n in range(blocks)], axis=0
        )
        high = stacked.astype(jnp.bfloat16)
        rest = stacked - high.astype(jnp.float32)
        middle = rest.astype(jnp.bfloat16)
        low = (rest - middle.astype(jnp.float32)).astype(jnp.bfloat16)
        within = jnp.dot(
            jnp.concatenate([high, middle, low], axis=1), after, preferred_element_type=jnp.float32
        )
        totals = jnp.sum(stacked, axis=1, keepdims=True)
        carried = jnp.zeros((HEADS, 1), jnp.float32)
        pieces = [None] * blocks
        for n in range(blocks - 1, -1, -1):
            pieces[n] = within[n * HEADS : (n + 1) * HEADS] + carried
            carried = carried + totals[n * HEADS : (n + 1) * HEADS]
        remain_after = jnp.concatenate(pieces, axis=1)
        weights = jnp.where(live, jnp.exp(scores + remain + remain_after), 0.0)
        mixed = jnp.dot(
            weights.astype(jnp.bfloat16), v_ref[item], preferred_element_type=jnp.float32
        )
        mixed = jnp.where(late, mixed[:, HEAD_DIM:], mixed[:, :HEAD_DIM])
        out_ref[item] = mixed.astype(jnp.bfloat16)


def stick_read(queries, key_cache, value_cache, lengths, head_bias):
    batch, span, lanes = key_cache.shape
    heads = queries.reshape(batch, HEADS, HEAD_DIM)
    each = min(4, batch)
    mixed = pl.pallas_call(
        stick_kernel,
        out_shape=jax.ShapeDtypeStruct((batch, HEADS, HEAD_DIM), jnp.bfloat16),
        grid=(batch // each,),
        in_specs=[
            pl.BlockSpec(memory_space=pltpu.SMEM),
            pl.BlockSpec((each, HEADS, HEAD_DIM), lambda i: (i, 0, 0)),
            pl.BlockSpec((each, span, lanes), lambda i: (i, 0, 0)),
            pl.BlockSpec((each, span, lanes), lambda i: (i, 0, 0)),
            pl.BlockSpec((HEADS, LANES), lambda i: (0, 0)),
        ],
        out_specs=pl.BlockSpec((each, HEADS, HEAD_DIM), lambda i: (i, 0, 0)),
        name="stick_read",
    )(lengths, heads, key_cache, value_cache, jnp.broadcast_to(head_bias[:, None], (HEADS, LANES)))
    return mixed.reshape(batch, HEADS * HEAD_DIM)


def shards(
    tokens,
    cache_keys,
    cache_values,
    cache_len,
    norm_gain_first,
    w_query,
    w_key,
    w_value,
    head_bias,
    w_output,
    norm_gain_second,
    group_id,
    member,
    group_gate,
    member_weight,
    expert_gate_w,
    expert_up_w,
    expert_down_w,
    dense_gate_w,
    dense_up_w,
    hidden_gain,
    dense_down_w,
    branch_logit,
):
    devices = lax.axis_size("ep")
    chips = devices // 2
    me = lax.axis_index("ep")
    first = lax.rem(me, 2) == 0
    partner = [(i, i + 1 - 2 * (i % 2)) for i in range(devices)]
    seq_dev, width = tokens.shape

    def both(own):
        other = lax.ppermute(own, "ep", partner)
        return jnp.where(
            first, jnp.concatenate([own, other], axis=-1), jnp.concatenate([other, own], axis=-1)
        )

    query_w = both(w_query)
    output_w = both(w_output)
    gate_w = both(dense_gate_w)
    up_w = both(dense_up_w)
    down_w = both(dense_down_w)

    stream = tokens.astype(jnp.float32)
    normed_first = (stream * rms_scale(stream) * norm_gain_first).astype(jnp.bfloat16)
    new_keys = jnp.dot(normed_first, w_key, preferred_element_type=jnp.float32).astype(jnp.bfloat16)
    new_values = jnp.dot(normed_first, w_value, preferred_element_type=jnp.float32).astype(
        jnp.bfloat16
    )
    queries = project(chips, 1, normed_first, query_w)
    attended = stick_read(queries, cache_keys, cache_values, cache_len, head_bias)
    projected = project(chips, 2, attended, output_w)
    second_stream = stream + projected.astype(jnp.float32)
    normed_second = (second_stream * rms_scale(second_stream) * norm_gain_second).astype(
        jnp.bfloat16
    )

    experts = devices * expert_gate_w.shape[0]
    capacity = seq_dev // (experts // PER_GROUP)
    notes = jnp.concatenate(
        [member, group_id[:, None], jnp.zeros((seq_dev, LANES - TOP_K - 1), jnp.int32)], axis=1
    ).astype(jnp.bfloat16)
    own_rows, own_notes, hidden = gather_rows(chips, 3, normed_second, notes, gate_w, up_w)
    other_rows = lax.ppermute(own_rows, "ep", partner)
    other_notes = lax.ppermute(own_notes, "ep", partner)
    dense_out = down_project(chips, 4, hidden, hidden_gain, down_w)

    def selection(rows_notes, parity):
        table = rows_notes[:, : TOP_K + 1].astype(jnp.int32)
        named = table[:, TOP_K :] * PER_GROUP + table[:, :TOP_K]
        hits = jnp.any(named == me, axis=1).reshape(chips, seq_dev)
        index = jnp.arange(seq_dev)
        earlier = (index[:, None] < index[None, :]).astype(jnp.float32)
        slot = jnp.dot(hits.astype(jnp.float32), earlier).astype(jnp.int32)
        spot = ((jnp.arange(chips)[:, None] * 2 + parity) * capacity + slot).reshape(-1)
        spot = jnp.where(hits.reshape(-1), spot, -1)
        return (jnp.arange(devices * capacity)[:, None] == spot[None, :]).astype(jnp.bfloat16)

    parity = lax.rem(me, 2)
    packed = jnp.dot(selection(own_notes, parity), own_rows, preferred_element_type=jnp.float32)
    packed = packed + jnp.dot(
        selection(other_notes, 1 - parity), other_rows, preferred_element_type=jnp.float32
    )
    packed = packed.astype(jnp.bfloat16)
    gate_pre = jnp.dot(packed, expert_gate_w[0], preferred_element_type=jnp.float32)
    upper_pre = jnp.dot(packed, expert_up_w[0], preferred_element_type=jnp.float32)
    expert_hidden = (jax.nn.silu(gate_pre) * upper_pre).astype(jnp.bfloat16)
    served = jnp.dot(expert_hidden, expert_down_w[0], preferred_element_type=jnp.float32).astype(
        jnp.bfloat16
    )
    returned = lax.all_to_all(
        served.reshape(devices, capacity, width), "ep", split_axis=0, concat_axis=0, tiled=True
    ).reshape(experts * capacity, width)

    pair_expert = (group_id[:, None] * PER_GROUP + member).reshape(-1)
    pair_count = pair_expert.shape[0]
    expert_hits = (pair_expert[:, None] == jnp.arange(experts, dtype=jnp.int32)[None, :]).astype(
        jnp.float32
    )
    earlier = (jnp.arange(pair_count)[:, None] > jnp.arange(pair_count)[None, :]).astype(
        jnp.float32
    )
    before = jnp.dot(earlier, expert_hits, preferred_element_type=jnp.float32)
    slot_index = jnp.sum(before * expert_hits, axis=1).astype(jnp.int32)
    target = pair_expert * capacity + slot_index
    select = (target[:, None] == jnp.arange(experts * capacity, dtype=jnp.int32)[None, :]).astype(
        jnp.bfloat16
    )
    pair_out = jnp.dot(select, returned, preferred_element_type=jnp.float32)
    combine = (group_gate[:, None] * member_weight).reshape(-1, 1)
    routed = jnp.sum((pair_out * combine).reshape(seq_dev, TOP_K, width), axis=1)
    mixed_out = (
        second_stream + routed + jax.nn.sigmoid(branch_logit) * dense_out.astype(jnp.float32)
    )
    return (mixed_out.astype(jnp.bfloat16), new_keys, new_values)


def solution(mesh):
    in_specs = (
        P("ep", None),
        P("ep", None, None),
        P("ep", None, None),
        P("ep"),
        P(),
        P(None, "ep"),
        P(),
        P(),
        P(),
        P(None, "ep"),
        P(),
        P("ep"),
        P("ep", None),
        P("ep"),
        P("ep", None),
        P("ep", None, None),
        P("ep", None, None),
        P("ep", None, None),
        P(None, "ep"),
        P(None, "ep"),
        P(),
        P(None, "ep"),
        P(),
    )
    out_specs = (P("ep", None), P("ep", None), P("ep", None))
    return jax.shard_map(shards, mesh=mesh, in_specs=in_specs, out_specs=out_specs, check_vma=False)
```

time: 333 us -> 174 us (0.52)
  waiting for transfers between devices: 194 us -> 1.13 us
  Pallas kernels: 0 us -> 113 us
  blocking collectives: 41.4 us -> 0 us
  matrix products: 40.2 us -> 15.3 us
  other arithmetic: 6.37 us -> 19.5 us
  between operations: 14.1 us -> 0.98 us
  local copies, waits for them, and re-layouts: 24.6 us -> 17.3 us
  starting transfers between devices: 10.9 us -> 5.86 us
    all_gather x4 -> x0, waiting for transfers between devices: 177 us -> none  [the longest x1 58.1 us: shards(): lax.all_gather(dense_down_w, 'ep', axis=1, tiled=True)]
    pallas_call x0 -> x5, Pallas kernels: none -> 113 us  [the longest x2 50.1 us: project(): pl.pallas_call(functools.partial(project_kernel, chips), out_shape=jax.Sh...]
    all_to_all x2 -> x0, blocking collectives: 41.4 us -> none  [the longest x1 30.7 us: shards(): lax.all_to_all(packed, 'ep', split_axis=0, concat_axis=0, tiled=True)]
    dot_general x13 -> x7, matrix products: 36.4 us -> 11.5 us  [the longest x1 4.23 us: shards(): jnp.dot(expert_hidden, expert_down_w[0], preferred_element_type=jnp.float32)]
    all_to_all x3 -> x1, waiting for transfers between devices: 17.4 us -> 0.01 us  [shards(): lax.all_to_all(served.reshape(devices, capacity, width), 'ep', split_axis...]
    select_n x0 -> x7, other arithmetic: none -> 14.1 us  [the longest x5 14 us: both(): jnp.where(first, jnp.concatenate([own, other], axis=-1), jnp.concatenate(...]
    unnamed x41 -> x35, local copies, waits for them, and re-layouts: 16.9 us -> 7.7 us
    all_to_all x3 -> x1, starting transfers between devices: 10.7 us -> 3.83 us  [shards(): lax.all_to_all(served.reshape(devices, capacity, width), 'ep', split_axis...]
  transfers between devices with their start and end apart: 7 -> 8, of which waited for: 7 -> 1; matrix products, arithmetic and copies ran while one was open for 10% -> 21% of each run, Pallas kernels for 0% -> 55%
where the time goes in v1:
time: 174 us; the launch traced here: 173 us
  Pallas kernels  113 us (65%)
  other arithmetic  19.5 us (11%)
  local copies, waits for them, and re-layouts  17.3 us (10%)
  matrix products  15.3 us (9%)
  starting transfers between devices  5.86 us (3%)
    pallas_call x2, Pallas kernels, project(): pl.pallas_call(functools.partial(project_kernel, chips), out_shape=jax.Sh...  50.1 us
    pallas_call x1, Pallas kernels, down_project(): pl.pallas_call(functools.partial(down_kernel, chips), out_shape=jax.Shape...  35.4 us
    pallas_call x1, Pallas kernels, gather_rows(): pl.pallas_call(functools.partial(gather_kernel, chips), out_shape=(jax.Sh...  18.1 us
    select_n x5, other arithmetic, both(): jnp.where(first, jnp.concatenate([own, other], axis=-1), jnp.concatenate(...  14 us
    pallas_call x1, Pallas kernels, stick_read(): pl.pallas_call(stick_kernel, out_shape=jax.ShapeDtypeStruct((batch, HEADS...  9.84 us
    unnamed x35, local copies, waits for them, and re-layouts  7.7 us
    dot_general x1, matrix products, shards(): jnp.dot(expert_hidden, expert_down_w[0], preferred_element_type=jnp.float32)  4.23 us
    all_to_all x1, starting transfers between devices, shards(): lax.all_to_all(served.reshape(devices, capacity, width), 'ep', split_axis...  3.83 us
  transfers between devices with their start and end apart: 8, of which 1 were waited for; matrix products, arithmetic and copies ran while one was open for 21% of the time, Pallas kernels for 55%

profile of v1, /device:TPU:0, one launch (start us, length us, event | category | flops | bytes accessed | tf_op | source)
XLA Modules:
  0.0 173.5 jit_solution(8889830614820188981)
XLA Ops:
  0.7 1.4 copy.96
  2.6 1.2 copy.93
  4.0 2.0 %copy.87 = bf16[2048,64]{1,0:T(8,128)(2,1)} copy(bf16[2048,64]{0,1:T(8,128)(2,1)} %param.32) | data formatting | bytes 524288 | tf_op args[9]
  8.6 1.1 collective-permute-done
  9.7 2.9 %maximum_select_fusion.w_ref = bf16[2048,128]{1,0:T(8,128)(2,1)} fusion(bf16[2048,64]{1,0:T(8,128)(2,1)} %collective-permute-done, bf16[2048,64]{1,0:T(8,128)(2,1)} %copy.84, pred[]{:T(512)S(6)} %eq.32), kind=kLoop, calls=%fused_computation.21 | loop fusion | flops 2359296 | bytes 1048577 | tf_op jit(solution)/shard_map/jit(_where)/select_n | solution.py:408
  12.6 28.6 %project.2 = bf16[16,2048]{1,0:T(8,128)(2,1)} custom-call(bf16[16,1024]{1,0:T(8,128)(2,1)} %get-tuple-element.16.a_ref, bf16[16,1024]{1,0:T(8,128)(2,1)} %get-tuple-element.15.b_ref, bf16[2048,128]{1,0:T(8,128)(2,1)} %maximum_select_fusion.w_ref), custom_call_target="tpu_custom_call" | custom-call | tf_op jit(solution)/shard_map/project/pallas_call | solution.py:257
  41.2 1.7 reshape.99.q_ref
  43.6 9.8 %stick_read.1 = bf16[16,32,64]{2,1,0:T(8,128)(2,1)} custom-call(s32[16]{0:T(128)} %lens_ref.1, bf16[16,32,64]{2,1,0:T(8,128)(2,1)} %reshape.99.q_ref, bf16[16,1024,128]{2,1,0:T(8,128)(2,1)} %k_ref.1, bf16[16,1024,128]{2,1,0:T(8,128)(2,1)} %v_ref.1, f32[32,128]{1,0:T(8,128)} %broadcast_in_dim.13.bias_ref), custom_call_target="tpu_custom_call" | custom-call | tf_op jit(solution)/shard_map/stick_read/pallas_call | solution.py:357
  55.1 3.0 %maximum_select_fusion.1.w_ref = bf16[2048,128]{1,0:T(8,128)(2,1)} fusion(bf16[2048,64]{1,0:T(8,128)(2,1)} %collective-permute-done.1, bf16[2048,64]{1,0:T(8,128)(2,1)} %copy.87, pred[]{:T(512)S(6)} %eq.32), kind=kLoop, calls=%fused_computation.22 | loop fusion | flops 2359296 | bytes 1048577 | tf_op jit(solution)/shard_map/jit(_where)/select_n | solution.py:408
  58.1 21.5 %project.3 = bf16[16,2048]{1,0:T(8,128)(2,1)} custom-call(bf16[16,1024]{1,0:T(8,128)(2,1)} %get-tuple-element.14.a_ref, bf16[16,1024]{1,0:T(8,128)(2,1)} %get-tuple-element.13.b_ref, bf16[2048,128]{1,0:T(8,128)(2,1)} %maximum_select_fusion.1.w_ref), custom_call_target="tpu_custom_call" | custom-call | tf_op jit(solution)/shard_map/project/pallas_call | solution.py:257
  82.8 2.6 %maximum_select_fusion.3.up_ref = bf16[2048,128]{1,0:T(8,128)(2,1)} fusion(bf16[2048,64]{1,0:T(8,128)(2,1)} %collective-permute-done.3, bf16[2048,64]{1,0:T(8,128)(2,1)S(1)} %copy.96, pred[]{:T(512)S(6)} %eq.32), kind=kLoop, calls=%fused_computation.24 | loop fusion | flops 2359296 | bytes 1048577 | tf_op jit(solution)/shard_map/jit(_where)/select_n | solution.py:408
  85.5 2.6 %maximum_select_fusion.2.gate_ref = bf16[2048,128]{1,0:T(8,128)(2,1)} fusion(bf16[2048,64]{1,0:T(8,128)(2,1)} %collective-permute-done.2, bf16[2048,64]{1,0:T(8,128)(2,1)S(1)} %copy.93, pred[]{:T(512)S(6)} %eq.32), kind=kLoop, calls=%fused_computation.23 | loop fusion | flops 2359296 | bytes 1048577 | tf_op jit(solution)/shard_map/jit(_where)/select_n | solution.py:408
  88.1 18.1 %gather_rows.1 = (bf16[256,2048]{1,0:T(8,128)(2,1)}, bf16[256,128]{1,0:T(8,128)(2,1)}, bf16[256,128]{1,0:T(8,128)(2,1)}) custom-call(bf16[16,1152]{1,0:T(8,128)(2,1)} %concatenate.40.a_ref, bf16[16,1024]{1,0:T(8,128)(2,1)} %get-tuple-element.11.b_ref, bf16[2048,128]{1,0:T(8,128)(2,1)} %maximum_select_fusion.2.gate_ref, ...), custom_call_target="tpu_custom_call" | custom-call | tf_op jit(solution)/shard_map/gather_rows/pallas_call | solution.py:273
  108.3 3.0 %fusion.25 = f32[256,2048]{1,0:T(8,128)} fusion(bf16[256,2048]{1,0:T(8,128)(2,1)} %get-tuple-element.7, s32[256]{0:T(256)S(1)} %broadcast_select_fusion.1), kind=kOutput, calls=%fused_computation.34 | convolution fusion | flops 268500992 | bytes 3146752 | tf_op jit(solution)/shard_map/dot_general | solution.py:454
  112.1 2.2 %fusion = bf16[256,2048]{1,0:T(8,128)(2,1)S(1)} fusion(f32[256,2048]{1,0:T(8,128)} %fusion.25, bf16[256,2048]{1,0:T(8,128)(2,1)S(1)} %collective-permute-done.5, s32[256]{0:T(256)S(1)} %broadcast_select_fusion), kind=kOutput, calls=%fused_computation.2 | convolution fusion | flops 269549568 | bytes 4195328 | tf_op jit(solution)/shard_map/dot_general | solution.py:455
  116.0 4.2 %fusion.1 = bf16[32,8,2048]{2,1,0:T(8,128)(2,1)} fusion(bf16[1,512,2048]{2,1,0:T(8,128)(2,1)S(1)} %copy-done, bf16[256,2048]{1,0:T(8,128)(2,1)} %copy-done.2, bf16[1,2048,512]{2,1,0:T(8,128)(2,1)} %param.39, f32[256,512]{1,0:T(8,128)S(1)} %fusion.5), kind=kOutput, calls=%fused_computation.3 | convolution fusion | flops 1075052544 | bytes 6815744 | tf_op jit(solution)/shard_map/dot_general | solution.py:462
  120.3 3.8 %all-to-all-start = ((bf16[32,8,2048]{2,1,0:T(8,128)(2,1)}), bf16[32,8,2048]{2,1,0:T(8,128)(2,1)S(1)}, u32[]{:S(2)}, u32[]{:S(2)}) async-start(bf16[32,8,2048]{2,1,0:T(8,128)(2,1)} %fusion.1), calls=%async_computation | async-start | bytes 2097152 | tf_op jit(solution)/shard_map/all_to_all | solution.py:465
  126.4 1.8 %convolution_convert_fusion.4 = bf16[16,128]{1,0:T(8,128)(2,1)} fusion(bf16[16,2048]{1,0:T(8,128)(2,1)S(1)} %fusion.28, bf16[2048,128]{1,0:T(8,128)(2,1)} %param.29), kind=kOutput, calls=%fused_computation.19 | convolution fusion | flops 8390656 | bytes 593920 | tf_op jit(solution)/shard_map/dot_general | solution.py:420
  128.2 1.8 %convolution_convert_fusion.3 = bf16[16,128]{1,0:T(8,128)(2,1)} fusion(bf16[16,2048]{1,0:T(8,128)(2,1)S(1)} %fusion.28, bf16[2048,128]{1,0:T(8,128)(2,1)} %param.30), kind=kOutput, calls=%fused_computation.18 | convolution fusion | flops 8390656 | bytes 593920 | tf_op jit(solution)/shard_map/dot_general | solution.py:421
  130.2 1.4 fusion.40
  131.6 3.0 %maximum_select_fusion.4.w_ref = bf16[2048,128]{1,0:T(8,128)(2,1)} fusion(bf16[2048,64]{1,0:T(8,128)(2,1)} %collective-permute-done.6, bf16[2048,64]{1,0:T(8,128)(2,1)} %copy.100, pred[]{:T(512)S(6)} %eq.32), kind=kLoop, calls=%fused_computation.25 | loop fusion | flops 2359296 | bytes 1048577 | tf_op jit(solution)/shard_map/jit(_where)/select_n | solution.py:408
  134.6 35.4 %down_project.1 = bf16[16,2048]{1,0:T(8,128)(2,1)} custom-call(bf16[128,128]{1,0:T(8,128)(2,1)} %get-tuple-element.10.a_ref, bf16[128,128]{1,0:T(8,128)(2,1)} %get-tuple-element.9.b_ref, f32[1,2048]{1,0:T(1,128)} %bitcast.33, bf16[2048,128]{1,0:T(8,128)(2,1)} %maximum_select_fusion.4.w_ref), custom_call_target="tpu_custom_call" | custom-call | tf_op jit(solution)/shard_map/down_project/pallas_call | solution.py:293
  170.0 1.2 convolution_multiply_fusion
  171.2 1.2 reshape.108
  (90 shorter events, 16.9 us)
Async XLA Ops:
  0.6 115.4 %copy-start = (bf16[1,512,2048]{2,1,0:T(8,128)(2,1)S(1)}, bf16[1,512,2048]{2,1,0:T(8,128)(2,1)}, u32[]{:S(2)}) copy-start(bf16[1,512,2048]{2,1,0:T(8,128)(2,1)} %param.40) | copy-start | bytes 6291460
  0.6 5.8 %copy-start.4 = (bf16[2048,64]{0,1:T(8,128)(2,1)S(1)}, bf16[2048,64]{0,1:T(8,128)(2,1)}, u32[]{:S(2)}) copy-start(bf16[2048,64]{0,1:T(8,128)(2,1)} %param.28) | copy-start | bytes 786436
  0.7 6.8 %copy-start.1 = (bf16[16,2048]{1,0:T(8,128)(2,1)S(1)}, bf16[16,2048]{1,0:T(8,128)(2,1)}, u32[]{:S(2)}) copy-start(bf16[16,2048]{1,0:T(8,128)(2,1)} %param.23) | copy-start | bytes 196612
  0.7 6.9 %copy-start.14 = (s32[16]{0:T(128)S(1)}, s32[16]{0:T(128)}, u32[]{:S(2)}) copy-start(s32[16]{0:T(128)} %param.34) | copy-start | bytes 196
  0.7 7.0 %copy-start.10 = (s32[16,6]{0,1:T(8,128)S(1)}, s32[16,6]{0,1:T(8,128)}, u32[]{:S(2)}) copy-start(s32[16,6]{0,1:T(8,128)} %param.35) | copy-start | bytes 1156
  0.7 7.0 %copy-start.7 = (f32[2048]{0:T(1024)S(1)}, f32[2048]{0:T(1024)}, u32[]{:S(2)}) copy-start(f32[2048]{0:T(1024)} %param.27) | copy-start | bytes 24580
  2.1 80.8 %collective-permute-start.3 = (bf16[2048,64]{1,0:T(8,128)(2,1)S(1)}, bf16[2048,64]{1,0:T(8,128)(2,1)}, u32[]{:S(2)}, u32[]{:S(2)}) collective-permute-start(bf16[2048,64]{1,0:T(8,128)(2,1)S(1)} %copy.96), channel_id=1, source_target_pairs={{0,1},{1,0},{2,3},{3,2},{4,5},{5,4},{6,7},{7,6},{8,9},{9,8},{10,11... | collective-permute-start | bytes 786440 | tf_op jit(solution)/shard_map/ppermute | solution.py:407
  3.9 39.0 %copy-start.12 = (f32[32]{0:T(128)S(1)}, f32[32]{0:T(128)}, u32[]{:S(2)}) copy-start(f32[32]{0:T(128)} %param.31) | copy-start | bytes 388
  3.9 81.6 %collective-permute-start.2 = (bf16[2048,64]{1,0:T(8,128)(2,1)S(1)}, bf16[2048,64]{1,0:T(8,128)(2,1)}, u32[]{:S(2)}, u32[]{:S(2)}) collective-permute-start(bf16[2048,64]{1,0:T(8,128)(2,1)S(1)} %copy.93), channel_id=1, source_target_pairs={{0,1},{1,0},{2,3},{3,2},{4,5},{5,4},{6,7},{7,6},{8,9},{9,8},{10,11... | collective-permute-start | bytes 786440 | tf_op jit(solution)/shard_map/ppermute | solution.py:407
  5.9 49.2 %collective-permute-start.1 = (bf16[2048,64]{1,0:T(8,128)(2,1)}, bf16[2048,64]{1,0:T(8,128)(2,1)}, u32[]{:S(2)}, u32[]{:S(2)}) collective-permute-start(bf16[2048,64]{1,0:T(8,128)(2,1)} %copy.87), channel_id=1, source_target_pairs={{0,1},{1,0},{2,3},{3,2},{4,5},{5,4},{6,7},{7,6},{8,9},{9,8},{10,11... | collective-permute-start | bytes 786440 | tf_op jit(solution)/shard_map/ppermute | solution.py:407
  7.4 2.3 %collective-permute-start = (bf16[2048,64]{1,0:T(8,128)(2,1)}, bf16[2048,64]{1,0:T(8,128)(2,1)}, u32[]{:S(2)}, u32[]{:S(2)}) collective-permute-start(bf16[2048,64]{1,0:T(8,128)(2,1)} %copy.84), channel_id=1, source_target_pairs={{0,1},{1,0},{2,3},{3,2},{4,5},{5,4},{6,7},{7,6},{8,9},{9,8},{10,11... | collective-permute-start | bytes 786440 | tf_op jit(solution)/shard_map/ppermute | solution.py:407
  53.4 27.2 %copy-start.8 = (f32[2048]{0:T(1024)S(1)}, f32[2048]{0:T(1024)}, u32[]{:S(2)}) copy-start(f32[2048]{0:T(1024)} %param.33) | copy-start | bytes 24580
  106.1 5.2 %collective-permute-start.4 = (bf16[256,128]{1,0:T(8,128)(2,1)}, bf16[256,128]{1,0:T(8,128)(2,1)S(1)}, u32[]{:S(2)}, u32[]{:S(2)}) collective-permute-start(bf16[256,128]{1,0:T(8,128)(2,1)} %get-tuple-element.6), channel_id=1, source_target_pairs={{0,1},{1,0},{2,3},{3,2},{4,5},{5,4},{6,7},{7,6},{8,9},{9,8},{10,11... | collective-permute-start | bytes 196616 | tf_op jit(solution)/shard_map/ppermute | solution.py:439
  107.8 4.3 %collective-permute-start.5 = (bf16[256,2048]{1,0:T(8,128)(2,1)}, bf16[256,2048]{1,0:T(8,128)(2,1)S(1)}, u32[]{:S(2)}, u32[]{:S(2)}) collective-permute-start(bf16[256,2048]{1,0:T(8,128)(2,1)} %get-tuple-element.7), channel_id=1, source_target_pairs={{0,1},{1,0},{2,3},{3,2},{4,5},{5,4},{6,7},{7,6},{8,9},{9,8},{10,11... | collective-permute-start | bytes 3145736 | tf_op jit(solution)/shard_map/ppermute | solution.py:438
  112.1 3.2 %copy-start.13 = (bf16[1,2048,512]{2,1,0:T(8,128)(2,1)S(1)}, bf16[1,2048,512]{2,1,0:T(8,128)(2,1)}, u32[]{:S(2)}) copy-start(bf16[1,2048,512]{2,1,0:T(8,128)(2,1)} %param.38) | copy-start | bytes 6291460
  114.3 1.0 copy-start.2
  120.2 3.8 %copy-start.5 = (bf16[2048,64]{0,1:T(8,128)(2,1)S(1)}, bf16[2048,64]{0,1:T(8,128)(2,1)}, u32[]{:S(2)}) copy-start(bf16[2048,64]{0,1:T(8,128)(2,1)} %param.44) | copy-start | bytes 786436
  120.2 5.5 %copy-start.11 = (f32[16,6]{0,1:T(8,128)S(1)}, f32[16,6]{0,1:T(8,128)}, u32[]{:S(2)}) copy-start(f32[16,6]{0,1:T(8,128)} %param.37) | copy-start | bytes 1156
  120.2 6.1 %copy-start.9 = (f32[2048]{0:T(1024)S(1)}, f32[2048]{0:T(1024)}, u32[]{:S(2)}) copy-start(f32[2048]{0:T(1024)} %param.45) | copy-start | bytes 24580
  120.3 49.7 %all-to-all-start = ((bf16[32,8,2048]{2,1,0:T(8,128)(2,1)}), bf16[32,8,2048]{2,1,0:T(8,128)(2,1)S(1)}, u32[]{:S(2)}, u32[]{:S(2)}) async-start(bf16[32,8,2048]{2,1,0:T(8,128)(2,1)} %fusion.1), calls=%async_computation | async-start | bytes 2097152 | tf_op jit(solution)/shard_map/all_to_all | solution.py:465
  125.1 6.5 %collective-permute-start.6 = (bf16[2048,64]{1,0:T(8,128)(2,1)}, bf16[2048,64]{1,0:T(8,128)(2,1)}, u32[]{:S(2)}, u32[]{:S(2)}) collective-permute-start(bf16[2048,64]{1,0:T(8,128)(2,1)} %copy.100), channel_id=1, source_target_pairs={{0,1},{1,0},{2,3},{3,2},{4,5},{5,4},{6,7},{7,6},{8,9},{9,8},{10,11... | collective-permute-start | bytes 786440 | tf_op jit(solution)/shard_map/ppermute | solution.py:407
  170.0 2.8 %copy-start.3 = (bf16[16,2048]{1,0:T(8,128)(2,1)S(1)}, bf16[16,2048]{1,0:T(8,128)(2,1)}, u32[]{:S(2)}) copy-start(bf16[16,2048]{1,0:T(8,128)(2,1)} %project.3) | copy-start | bytes 196612
  170.0 2.8 %copy-start.6 = (bf16[16,2048]{1,0:T(8,128)(2,1)S(1)}, bf16[16,2048]{1,0:T(8,128)(2,1)}, u32[]{:S(2)}) copy-start(bf16[16,2048]{1,0:T(8,128)(2,1)} %down_project.1) | copy-start | bytes 196612
